TPU v7x, 32 devices: a whole 2x2x4 slice. The times are simulated.
32 devices in a mesh: sp: 16 (over z, y, x), dp: 2 (over core).
Axes of the slice: x: 2, y: 2, z: 4, core: 2. Of those that a mesh axis runs over, the one named last changes fastest.
Arguments:
- inputs: bfloat16 [2, 2048, 2048], P('dp', 'sp'), may hold values from -6 to 6
- conv_weight: bfloat16 [4, 2048], replicated, may hold values from -3 to 3
- gate_weight: bfloat16 [2, 8, 256, 256], P(None, 'dp'), may hold values from -0.375 to 0.375
- rate_param: float32 [2048], replicated, may hold values from 4 to 12.5
- pace: float32 [2, 2048], P('dp'), may hold values from 0.5 to 30000
Outputs:
- recurrent: bfloat16 [2, 2048, 2048], P('dp', 'sp')
All inputs are finite; a program needn't handle non-finite values.
Results may differ from a plain program's by a relative error of at most 0.008.
Values may be sent and summed in bfloat16 or wider, within the bound.
A program may use at most 128 MiB of HBM per device.

v0:
```python
import jax
import jax.numpy as jnp
from jax import lax
from jax.sharding import PartitionSpec as P

HEADS = 8
BLOCK = 256
CONV = 4


gate_power = 8.0


def passed_along(array, axis, by):
    devices = lax.axis_size(axis)
    pairs = [(i, i + by) for i in range(devices) if 0 <= i + by < devices]
    return lax.ppermute(array, axis, pairs)


def combine(earlier, later):
    decay_e, state_e = earlier
    decay_l, state_l = later
    return (decay_e * decay_l, decay_l * state_e + state_l)


def lru_terms(pre_recur, pre_input, values, rate_col, pace_col):
    recur_gate = jax.nn.sigmoid(pre_recur.astype(jnp.float32))
    input_gate = jax.nn.sigmoid(pre_input.astype(jnp.float32))
    log_decay = -gate_power * pace_col * recur_gate * jax.nn.softplus(-rate_col)
    decay = jnp.exp(log_decay)
    drive = jnp.sqrt(-jnp.expm1(2.0 * log_decay)) * input_gate * values.astype(jnp.float32)
    return (decay, drive)


def body(inputs, conv_weight, gate_weight, rate_param, pace):
    own_rows = inputs[0].T
    width = own_rows.shape[0]
    count = own_rows.shape[1]
    earlier = passed_along(own_rows[:, count - (CONV - 1) :], "sp", 1)
    padded = jnp.concatenate([earlier, own_rows], axis=1).astype(jnp.float32)
    conv_taps = conv_weight.astype(jnp.float32)
    conv_out = jnp.zeros((width, count), jnp.float32)
    for tap in range(CONV):
        conv_out = conv_out + conv_taps[tap][:, None] * padded[:, tap : tap + count]
    conv_out = conv_out.astype(jnp.bfloat16)
    by_head = conv_out.reshape(HEADS, BLOCK, count)
    preact = (
        jnp.einsum(
            "hit,ghij->ghjt",
            by_head,
            lax.all_gather(gate_weight, "dp", axis=1, tiled=True),
            preferred_element_type=jnp.float32,
        )
        .astype(jnp.bfloat16)
        .reshape(2, width, count)
    )
    stacked = jnp.stack([conv_out, preact[0], preact[1]])
    arrived = lax.all_to_all(stacked, "sp", split_axis=1, concat_axis=2, tiled=True)
    lanes = arrived.shape[1]
    lane_rates = lax.dynamic_slice_in_dim(rate_param, lax.axis_index("sp") * lanes, lanes)
    decay, drive = lru_terms(
        arrived[1], arrived[2], arrived[0], lane_rates[:, None], pace[0][None, :]
    )
    _, state = lax.associative_scan(combine, (decay, drive), axis=1)
    result = lax.all_to_all(
        state.astype(jnp.bfloat16), "sp", split_axis=1, concat_axis=0, tiled=True
    )
    return result.T[None]


def solution(mesh):
    return jax.shard_map(
        body,
        mesh=mesh,
        in_specs=(P("dp", "sp", None), P(), P(None, "dp", None, None), P(), P("dp", None)),
        out_specs=P("dp", "sp", None),
        check_vma=False,
    )
```

profile of v0, /device:TPU:0, one launch (start us, length us, event | category | flops | bytes accessed | tf_op | source)
XLA Modules:
  0.0 151.2 jit_solution(12866272480589293699)
XLA Ops:
  6.5 0.0 all-gather.2.cloned.1.call-start
  6.5 2.3 %copy.31 = bf16[2,4,256,256]{3,2,0,1:T(8,128)(2,1)} copy(bf16[2,4,256,256]{3,2,1,0:T(8,128)(2,1)} %param.7) | data formatting | bytes 2097152 | tf_op args[2]
  8.9 0.0 all-gather.2.cloned.1.call-update
  8.9 0.0 copy-done.2
  8.9 0.3 copy.30
  9.2 0.2 slice.406
  9.4 4.9 %collective-permute-start = (bf16[2048,3]{1,0:T(8,128)(2,1)S(1)}, bf16[2048,3]{1,0:T(8,128)(2,1)S(1)}, u32[]{:S(2)}, u32[]{:S(2)}) collective-permute-start(bf16[2048,3]{1,0:T(8,128)(2,1)S(1)} %slice.406), channel_id=1, source_target_pairs={{0,2},{2,4},{4,6},{6,8},{8,10},{10,12},{12,14},{14,16},{16,18},{18... | collective-permute-start | bytes 36872 | tf_op jit(solution)/shard_map/ppermute | solution.py:17
  14.3 0.0 copy-done.3
  14.4 11.1 %collective-permute-done = bf16[2048,3]{1,0:T(8,128)(2,1)S(1)} collective-permute-done((bf16[2048,3]{1,0:T(8,128)(2,1)S(1)}, bf16[2048,3]{1,0:T(8,128)(2,1)S(1)}, u32[]{:S(2)}, u32[]{:S(2)}) %collective-permute-start) | collective-permute-done | bytes 12320 | tf_op jit(solution)/shard_map/ppermute | solution.py:17
  25.4 0.4 maximum_convert_fusion
  25.9 2.2 %fusion.29 = bf16[1,2048,128]{2,1,0:T(8,128)(2,1)S(1)} fusion(f32[2048,131]{1,0:T(8,128)S(1)} %maximum_convert_fusion, f32[2048]{0:T(1024)S(1)} %bitcast.61, f32[2048]{0:T(1024)S(1)} %bitcast.59, f32[2048]{0:T(1024)S(1)} %bitcast.57, f32[2048]{0:T(1024)S(1)} %bitcast.55), kind=kLoop, calls=%fused_computation.75 | loop fusion | flops 2097152 | bytes 4751360 | tf_op jit(solution)/shard_map/stack | solution.py:57
  28.0 2.2 %fusion.2 = bf16[2048,128]{1,0:T(8,128)(2,1)S(1)} fusion(f32[2048,131]{1,0:T(8,128)S(1)} %maximum_convert_fusion, f32[2048]{0:T(1024)S(1)} %bitcast.62, f32[2048]{0:T(1024)S(1)} %bitcast.60, f32[2048]{0:T(1024)S(1)} %bitcast.58, f32[2048]{0:T(1024)S(1)} %bitcast.56), kind=kLoop, calls=%fused_computation.5 | loop fusion | flops 2097152 | bytes 4751360 | tf_op jit(solution)/shard_map/convert_element_type | solution.py:45
  30.2 0.0 all-gather.2.cloned.1.call-done
  30.2 2.1 %fusion = bf16[2,8,256,128]{2,3,0,1:T(8,128)(2,1)S(1)} fusion(bf16[8,256,128,1]{2,1,3,0:T(8,128)(2,1)S(1)} %bitcast.49, bf16[2,8,256,256]{3,2,0,1:T(8,128)(2,1)} %all-gather.2.cloned.1.call-done), kind=kOutput, calls=%fused_computation.2 | convolution fusion | flops 268959744 | bytes 3670016 | tf_op jit(solution)/shard_map/hit,ghij->ghjt/dot_general | solution.py:48
  32.3 0.1 fusion.14
  32.4 0.3 copy.33
  32.7 0.3 copy.34
  33.0 0.2 pad_maximum_fusion
  33.1 10.7 %copy.35 = bf16[3,2048,128]{2,0,1:T(4,128)(2,1)} copy(bf16[3,2048,128]{2,1,0:T(8,128)(2,1)S(1)} %pad_maximum_fusion) | data formatting | bytes 3145728 | tf_op jit(solution)/shard_map/stack | solution.py:57
  43.9 8.0 %all-to-all-start = ((bf16[3,2048,128]{2,0,1:T(4,128)(2,1)}), bf16[3,2048,128]{2,0,1:T(4,128)(2,1)S(1)}, u32[]{:S(2)}, u32[]{:S(2)}) async-start(bf16[3,2048,128]{2,0,1:T(4,128)(2,1)} %copy.35), calls=%async_computation | async-start | bytes 4194304 | tf_op jit(solution)/shard_map/all_to_all | solution.py:58
  51.9 0.8 compare_select_fusion
  52.6 0.0 copy-done.4
  52.7 41.6 %all-to-all-done = bf16[3,2048,128]{2,0,1:T(4,128)(2,1)S(1)} async-done(((bf16[3,2048,128]{2,0,1:T(4,128)(2,1)}), bf16[3,2048,128]{2,0,1:T(4,128)(2,1)S(1)}, u32[]{:S(2)}, u32[]{:S(2)}) %all-to-all-start) | async-done | bytes 1572896 | tf_op jit(solution)/shard_map/all_to_all | solution.py:58
  94.3 0.2 copy.36
  94.5 0.1 slice_convert_fusion
  94.6 0.6 add_divide_fusion.1
  95.2 1.3 copy.39
  96.5 1.4 copy.37
  97.8 1.3 copy.38
  99.2 0.0 copy-done
  99.2 2.4 %fusion.6 = (f32[128,2048]{0,1:T(8,128)S(1)}, f32[128,2048]{0,1:T(8,128)S(1)}) fusion(f32[1,128,16,128]{1,3,2,0:T(8,128)} %copy.37, f32[128]{0:T(128)S(1)} %compare_select_fusion, f32[2048]{0:T(1024)S(1)} %bitcast.63, f32[1,128,16,128]{1,3,2,0:T(8,128)S(1)} %copy-done, f32[1,128,16,128]{1,3,2,0:T(8,128)} %copy.38), kind=kLoop, calls=%fused_computation.19 | loop fusion | flops 1572864 | bytes 5251584 | tf_op jit(solution)/shard_map/exp | solution.py:30
  101.6 0.7 slice.328
  102.3 2.1 %slice.324 = f32[128,1024]{0,1:T(8,128)} slice(f32[128,2048]{0,1:T(8,128)S(1)} %get-tuple-element.7), slice={[0:128:1], [1:2048:2]} | slice | bytes 1048576 | tf_op jit(solution)/shard_map/slice | solution.py:64
  104.4 0.7 slice.323
  105.1 0.0 copy-start.1
  105.1 0.7 slice.404
  105.8 2.0 %slice.326 = f32[128,1024]{0,1:T(8,128)} slice(f32[128,2048]{0,1:T(8,128)S(1)} %get-tuple-element.8), slice={[0:128:1], [1:2048:2]} | slice | bytes 1048576 | tf_op jit(solution)/shard_map/slice | solution.py:64
  107.8 2.0 %slice.325 = f32[128,1024]{0,1:T(8,128)} slice(f32[128,2048]{0,1:T(8,128)S(1)} %get-tuple-element.8), slice={[0:128:1], [0:2047:2]} | slice | bytes 1048576 | tf_op jit(solution)/shard_map/slice | solution.py:64
  109.9 0.0 copy-done.1
  109.9 1.3 fusion.15
  111.2 0.4 slice.334
  111.6 0.4 slice.330
  112.0 0.4 slice.329
  112.4 0.4 slice.402
  112.8 0.4 slice.332
  113.2 1.4 slice.331
  114.6 1.0 fusion.16
  115.6 0.1 slice.340
  115.7 0.1 slice.336
  115.8 0.3 slice.335
  116.1 0.3 slice.400
  116.4 0.1 slice.338
  116.5 0.1 slice.337
  118.2 0.1 fusion.8
  118.3 0.1 pad.85
  118.4 0.1 pad.86
  118.5 0.1 add.207
  118.5 0.1 fusion.7
  118.7 0.1 pad.87
  118.8 0.1 pad.88
  118.9 0.1 add_convert_fusion
  119.0 24.0 %all_to_all.34 = bf16[128,16,128]{0,2,1:T(8,128)(2,1)S(1)} all-to-all(bf16[128,16,128]{0,2,1:T(8,128)(2,1)S(1)} %bitcast.50), channel_id=1, replica_groups=mesh['sp'=16,'dp'=2] {'sp'}, dimensions={1} | all-to-all | bytes 1048576 | tf_op jit(solution)/shard_map/all_to_all | solution.py:65
  143.1 0.3 copy.40
  143.3 1.0 copy.41
  (107 shorter events, 1.3 us)
Async XLA Ops:
  6.5 2.4 %copy-start.2 = (bf16[1,128,2048]{2,1,0:T(8,128)(2,1)S(1)}, bf16[1,128,2048]{2,1,0:T(8,128)(2,1)}, u32[]{:S(2)}) copy-start(bf16[1,128,2048]{2,1,0:T(8,128)(2,1)} %param.5) | copy-start | bytes 1572868
  6.5 23.7 %all-gather.2.cloned.1.call-start = ((), (), s32[]{:S(2)}) async-start(), calls=%async_computation.2 | async-start | bytes 3145728 | tf_op jit(solution)/shard_map/all_gather | solution.py:51
  8.9 5.4 %copy-start.3 = (bf16[4,2048]{1,0:T(4,128)(2,1)S(1)}, bf16[4,2048]{1,0:T(4,128)(2,1)}, u32[]{:S(2)}) copy-start(bf16[4,2048]{1,0:T(4,128)(2,1)} %param.6) | copy-start | bytes 49156
  9.4 16.0 %collective-permute-start = (bf16[2048,3]{1,0:T(8,128)(2,1)S(1)}, bf16[2048,3]{1,0:T(8,128)(2,1)S(1)}, u32[]{:S(2)}, u32[]{:S(2)}) collective-permute-start(bf16[2048,3]{1,0:T(8,128)(2,1)S(1)} %slice.406), channel_id=1, source_target_pairs={{0,2},{2,4},{4,6},{6,8},{8,10},{10,12},{12,14},{14,16},{16,18},{18... | collective-permute-start | bytes 36872 | tf_op jit(solution)/shard_map/ppermute | solution.py:17
  43.9 8.8 %copy-start.4 = (f32[1,2048]{1,0:T(1,128)S(1)}, f32[1,2048]{1,0:T(1,128)}, u32[]{:S(2)}) copy-start(f32[1,2048]{1,0:T(1,128)} %param.9) | copy-start | bytes 24580
  43.9 50.4 %all-to-all-start = ((bf16[3,2048,128]{2,0,1:T(4,128)(2,1)}), bf16[3,2048,128]{2,0,1:T(4,128)(2,1)S(1)}, u32[]{:S(2)}, u32[]{:S(2)}) async-start(bf16[3,2048,128]{2,0,1:T(4,128)(2,1)} %copy.35), calls=%async_computation | async-start | bytes 4194304 | tf_op jit(solution)/shard_map/all_to_all | solution.py:58
  96.5 2.7 %copy-start = (f32[1,128,16,128]{1,3,2,0:T(8,128)S(1)}, f32[1,128,16,128]{1,3,2,0:T(8,128)}, u32[]{:S(2)}) copy-start(f32[1,128,16,128]{1,3,2,0:T(8,128)} %copy.39) | copy-start | bytes 3145732
  105.1 4.8 %copy-start.1 = (f32[128,1024]{0,1:T(8,128)S(1)}, f32[128,1024]{0,1:T(8,128)}, u32[]{:S(2)}) copy-start(f32[128,1024]{0,1:T(8,128)} %slice.324) | copy-start | bytes 1572868
Sparse Core Ops, SparseCore 0:
  9.0 13.2 all-gather.1
where the time goes:
time: 152 us; the launch traced here: 151 us
  waiting for transfers between devices  52.7 us (35%)
  local copies, waits for them, and re-layouts  33.3 us (22%)
  blocking collectives  24 us (16%)
  between operations  14.2 us (9%)
  starting transfers between devices  12.9 us (8%)
  other arithmetic  11.8 us (8%)
  matrix products  2.09 us (1%)
    all_to_all x1, waiting for transfers between devices, body(): lax.all_to_all(stacked, 'sp', split_axis=1, concat_axis=2, tiled=True)  41.6 us
    all_to_all x1, blocking collectives, body(): lax.all_to_all(state.astype(jnp.bfloat16), 'sp', split_axis=1, concat_axi...  24 us
    slice x67, local copies, waits for them, and re-layouts, body(): _, state = lax.associative_scan(combine, (decay, drive), axis=1)  13.2 us
    ppermute x1, waiting for transfers between devices, passed_along(): return lax.ppermute(array, axis, pairs)  11.1 us
    another operation x1, local copies, waits for them, and re-layouts, body(): stacked = jnp.stack([conv_out, preact[0], preact[1]])  10.7 us
    all_to_all x1, starting transfers between devices, body(): lax.all_to_all(stacked, 'sp', split_axis=1, concat_axis=2, tiled=True)  8 us
    ppermute x1, starting transfers between devices, passed_along(): return lax.ppermute(array, axis, pairs)  4.9 us
  transfers between devices with their start and end apart: 3, of which 2 were waited for; matrix products, arithmetic and copies ran while one was open for 4% of the time, Pallas kernels for 0%

commit v1 on v0

v1 whole, which is shorter than its diff:
```python
import functools
import math

import jax
import jax.numpy as jnp
from jax import lax
from jax.experimental import pallas as pl
from jax.experimental.pallas import tpu as pltpu
from jax.sharding import PartitionSpec as P

CONV = 4
gate_power = 8.0
SUB = 8
LANES = 128
PIECE = SUB * LANES
TINY = 1.2e-38
LN2 = math.log(2.0)
SMALL = 0.07
MESH = pl.DeviceIdType.MESH


def softplus_neg(rate):
    e = jnp.exp(-jnp.abs(rate))
    series = e * (1.0 + e * (-0.5 + e * (1.0 / 3.0 + e * (-0.25 + e * 0.2))))
    return jnp.maximum(-rate, 0.0) + jnp.where(e < 0.03, series, jnp.log(1.0 + e))


def kernel(
    nsp, ndp, heads, block,
    x_hbm, cw_hbm, w_hbm, rate_hbm, pace_hbm, out_ref,
    x, cw, w, rate, pace_row, pace_mat, pace_perm, halo,
    hloc, acum, ex_h, ex_a, stage, send_buf, recv_buf, carry,
    load_sem, w_send, w_recv, halo_send, halo_recv, c_send, c_recv,
):
    me = lax.axis_index("sp")
    d = lax.axis_index("dp")
    count, width = x.shape
    steps = count // SUB
    hl = heads // ndp
    pieces = width // PIECE
    per = PIECE // block
    tiles = block // LANES

    barrier = pltpu.get_barrier_semaphore()

    @pl.loop(1, nsp)
    def _(o):
        pl.semaphore_signal(barrier, inc=1, device_id={"sp": lax.rem(me + o, nsp)}, device_id_type=MESH)

    @pl.loop(1, ndp)
    def _(o):
        pl.semaphore_signal(barrier, inc=1, device_id={"dp": lax.rem(d + o, ndp)}, device_id_type=MESH)

    first = pl.multiple_of(me * count, count)
    loads = [
        pltpu.make_async_copy(x_hbm.at[0], x, load_sem.at[0]),
        pltpu.make_async_copy(w_hbm, w.at[:, pl.ds(0, hl)], load_sem.at[1]),
        pltpu.make_async_copy(cw_hbm, cw, load_sem.at[2]),
        pltpu.make_async_copy(rate_hbm, rate, load_sem.at[3]),
        pltpu.make_async_copy(pace_hbm.at[:, pl.ds(first, count)], pace_row, load_sem.at[4]),
    ]
    for load in loads:
        load.start()

    @pl.when(me == 0)
    def _():
        halo[...] = jnp.zeros_like(halo)

    pl.semaphore_wait(barrier, nsp - 1 + ndp - 1)

    w_copies = []
    for o in range(1, ndp):
        w_copies.append(pltpu.make_async_remote_copy(
            src_ref=w_hbm,
            dst_ref=w.at[:, pl.ds(o * hl, hl)],
            send_sem=w_send.at[o],
            recv_sem=w_recv.at[o],
            device_id={"dp": lax.rem(d - o + ndp, ndp)},
            device_id_type=MESH,
        ))
    loads[0].wait()
    halo_copy = pltpu.make_async_remote_copy(
        src_ref=x.at[pl.ds(count - SUB, SUB)],
        dst_ref=halo,
        send_sem=halo_send.at[0],
        recv_sem=halo_recv.at[0],
        device_id={"sp": lax.rem(me + 1, nsp)},
        device_id_type=MESH,
    )

    @pl.when(me < nsp - 1)
    def _():
        halo_copy.start()

    for copy in w_copies:
        copy.start()
    for load in loads[1:]:
        load.wait()

    spread = jnp.broadcast_to(pace_row[...], (LANES, count)).T
    pace_mat[...] = spread
    for j in range(steps):
        pace_perm[j] = pace_mat[pl.ds(j, SUB, stride=steps), :]

    row = lax.broadcasted_iota(jnp.int32, (count, count), 0)
    col = lax.broadcasted_iota(jnp.int32, (count, count), 1)
    gather = jnp.where(col == (row % SUB) * steps + row // SUB, 1.0, 0.0).astype(jnp.bfloat16)
    scatter = jnp.where(row == (col % SUB) * steps + col // SUB, 1.0, 0.0).astype(jnp.bfloat16)
    sub = lax.broadcasted_iota(jnp.int32, (SUB, block), 0)

    @pl.when(me > 0)
    def _():
        halo_copy.wait_recv()

    def carry_copy(piece, src, dst):
        return pltpu.make_async_remote_copy(
            src_ref=send_buf.at[piece],
            dst_ref=recv_buf.at[src, piece],
            send_sem=c_send.at[dst, piece],
            recv_sem=c_recv.at[src, piece],
            device_id={"sp": dst},
            device_id_type=MESH,
        )

    def one_slot(piece, at):
        slot = piece * per + at
        off = pl.multiple_of(lax.rem(d * hl + slot, heads) * block, block)
        here = pl.ds(off, block)
        xp = jnp.dot(gather, x[:, here], preferred_element_type=jnp.float32)
        before = halo[:, here].astype(jnp.float32)
        taps = cw[:, here].astype(jnp.float32)
        taps = [jnp.broadcast_to(taps[k : k + 1], (SUB, block)) for k in range(CONV)]
        rows = [xp[SUB * j : SUB * (j + 1)] for j in range(steps)]
        early = []
        for m in range(CONV - 1, 0, -1):
            rolled = pltpu.roll(rows[steps - m], 1, 0)
            edge = jnp.broadcast_to(before[SUB - m : SUB - m + 1], (SUB, block))
            early.append(jnp.where(sub == 0, edge, rolled))
        rows = early + rows
        conv = []
        for j in range(steps):
            total = taps[0] * rows[j]
            for k in range(1, CONV):
                total = total + taps[k] * rows[j + k]
            conv.append(total)
        conv = jnp.concatenate(conv, axis=0).astype(jnp.bfloat16)
        pre_r = jnp.dot(conv, w[0, slot], preferred_element_type=jnp.float32)
        pre_i = jnp.dot(conv, w[1, slot], preferred_element_type=jnp.float32)
        pre_r = pre_r.astype(jnp.bfloat16).astype(jnp.float32)
        pre_i = pre_i.astype(jnp.bfloat16).astype(jnp.float32)
        values = conv.astype(jnp.float32)
        factor = softplus_neg(rate[:, here]) * (gate_power / LN2)
        factor = jnp.broadcast_to(factor, (SUB, block))
        h = None
        for j in range(steps):
            part = slice(SUB * j, SUB * (j + 1))
            pace_j = pace_perm[j]
            pace_j = jnp.concatenate([pace_j] * tiles, axis=1)
            r = 1.0 / (1.0 + jnp.exp(-pre_r[part]))
            i = 1.0 / (1.0 + jnp.exp(-pre_i[part]))
            q = pace_j * factor * r
            a = jnp.exp2(-q)
            c = 2.0 * LN2
            series = q * (c + q * (-c * c / 2 + q * (c**3 / 6 - q * (c**4 / 24))))
            gain = jnp.where(q < SMALL, series, 1.0 - a * a)
            b = gain * lax.rsqrt(jnp.maximum(gain, TINY)) * i * values[part]
            if h is None:
                h, total_a = b, a
            else:
                h = a * h + b
                total_a = total_a * a
            hloc[slot, part] = h
            acum[slot, part] = total_a
        for shift in (1, 2, 4):
            inside = sub >= shift
            earlier_a = jnp.where(inside, pltpu.roll(total_a, shift, 0), 1.0)
            earlier_h = jnp.where(inside, pltpu.roll(h, shift, 0), 0.0)
            h = total_a * earlier_h + h
            total_a = total_a * earlier_a
        ex_h[slot] = jnp.where(sub >= 1, pltpu.roll(h, 1, 0), 0.0)
        ex_a[slot] = jnp.where(sub >= 1, pltpu.roll(total_a, 1, 0), 1.0)
        log_a = jnp.log2(jnp.maximum(total_a, TINY))
        for t in range(tiles):
            lanes = slice(LANES * t, LANES * (t + 1))
            stage[pl.ds(at * tiles + t, 1), :] = log_a[SUB - 1 :, lanes]
            stage[pl.ds(SUB + at * tiles + t, 1), :] = h[SUB - 1 :, lanes]

    for piece in range(pieces):
        for o in range(1, ndp):
            if piece * per <= o * hl < (piece + 1) * per:
                w_copies[o - 1].wait_recv()

        @pl.loop(0, per)
        def _(at):
            one_slot(piece, at)

        send_buf[piece] = stage[...].astype(jnp.bfloat16)

        @pl.loop(me + 1, nsp)
        def _(dst):
            carry_copy(piece, me, dst).start()

    def finish_slot(piece, at):
        slot = piece * per + at
        off = pl.multiple_of(lax.rem(d * hl + slot, heads) * block, block)
        start = jnp.concatenate(
            [
                jnp.broadcast_to(carry[pl.ds(at * tiles + t, 1), :], (SUB, LANES))
                for t in range(tiles)
            ],
            axis=1,
        )
        start = ex_h[slot] + ex_a[slot] * start
        states = [
            hloc[slot, SUB * j : SUB * (j + 1)] + acum[slot, SUB * j : SUB * (j + 1)] * start
            for j in range(steps)
        ]
        states = jnp.concatenate(states, axis=0).astype(jnp.bfloat16)
        placed = jnp.dot(scatter, states, preferred_element_type=jnp.float32)
        out_ref[0, :, pl.ds(off, block)] = placed.astype(jnp.bfloat16)

    for piece in range(pieces):
        carry[...] = jnp.zeros_like(carry)

        @pl.loop(0, me)
        def _(src):
            carry_copy(piece, src, me).wait_recv()
            got = recv_buf[src, piece].astype(jnp.float32)
            carry[...] = jnp.exp2(got[:SUB]) * carry[...] + got[SUB:]

        @pl.loop(0, per)
        def _(at):
            finish_slot(piece, at)

    for copy in w_copies:
        copy.wait_send()

    @pl.when(me < nsp - 1)
    def _():
        halo_copy.wait_send()

    for piece in range(pieces):

        @pl.loop(me + 1, nsp)
        def _(dst):
            carry_copy(piece, me, dst).wait_send()


def body(inputs, conv_weight, gate_weight, rate_param, pace):
    nsp = lax.axis_size("sp")
    ndp = lax.axis_size("dp")
    _, count, width = inputs.shape
    block = gate_weight.shape[-1]
    heads = width // block
    pieces = width // PIECE
    f32, bf16 = jnp.float32, jnp.bfloat16
    anywhere = pl.BlockSpec(memory_space=pl.ANY)
    dma = pltpu.SemaphoreType.DMA
    return pl.pallas_call(
        functools.partial(kernel, nsp, ndp, heads, block),
        out_shape=jax.ShapeDtypeStruct(inputs.shape, bf16),
        in_specs=[anywhere] * 5,
        out_specs=pl.BlockSpec(memory_space=pltpu.VMEM),
        scratch_shapes=[
            pltpu.VMEM((count, width), bf16),
            pltpu.VMEM(conv_weight.shape, bf16),
            pltpu.VMEM((2, heads, block, block), bf16),
            pltpu.VMEM((1, width), f32),
            pltpu.VMEM((1, count), f32),
            pltpu.VMEM((count, LANES), f32),
            pltpu.VMEM((count // SUB, SUB, LANES), f32),
            pltpu.VMEM((SUB, width), bf16),
            pltpu.VMEM((heads, count, block), f32),
            pltpu.VMEM((heads, count, block), f32),
            pltpu.VMEM((heads, SUB, block), f32),
            pltpu.VMEM((heads, SUB, block), f32),
            pltpu.VMEM((2 * SUB, LANES), f32),
            pltpu.VMEM((pieces, 2 * SUB, LANES), bf16),
            pltpu.VMEM((nsp, pieces, 2 * SUB, LANES), bf16),
            pltpu.VMEM((SUB, LANES), f32),
            dma((5,)),
            dma((ndp,)),
            dma((ndp,)),
            dma((1,)),
            dma((1,)),
            dma((nsp, pieces)),
            dma((nsp, pieces)),
        ],
        compiler_params=pltpu.CompilerParams(collective_id=0, has_side_effects=True),
    )(inputs, conv_weight, gate_weight, rate_param.reshape(1, width), pace)


def solution(mesh):
    return jax.shard_map(
        body,
        mesh=mesh,
        in_specs=(P("dp", "sp", None), P(), P(None, "dp", None, None), P(), P("dp", None)),
        out_specs=P("dp", "sp", None),
        check_vma=False,
    )
```

time: 152 us -> 19.5 us (0.13)
  the two profiles are of different devices: /device:TPU:0 before, /device:TPU:24 now
where the time goes in v1:
time: 19.5 us; the launch traced here: 19.3 us
  Pallas kernels  17.4 us (89%)
  local copies, waits for them, and re-layouts  1.88 us (10%)
    pallas_call x1, Pallas kernels, body(): pl.pallas_call(functools.partial(kernel, nsp, ndp, heads, block), out_sha...  17.4 us
    unnamed x1, local copies, waits for them, and re-layouts  1.88 us

profile of v1, /device:TPU:24, one launch (start us, length us, event | category | flops | bytes accessed | tf_op | source)
XLA Modules:
  0.0 19.3 jit_solution(9252874869252160071)
XLA Ops:
  0.0 17.4 %shard_map.55 = bf16[1,128,2048]{2,1,0:T(8,128)(2,1)} custom-call(bf16[1,128,2048]{2,1,0:T(8,128)(2,1)} %x_hbm.1, bf16[4,2048]{1,0:T(4,128)(2,1)} %cw_hbm.1, bf16[2,4,256,256]{3,2,1,0:T(8,128)(2,1)} %w_hbm.1, f32[1,2048]{1,0:T(1,128)} %bitcast.1, f32[1,2048]{1,0:T(1,128)} %pace_hbm.1), custom_call_target="tpu_custom_call" | custom-call | tf_op jit(solution)/shard_map/pallas_call | solution.py:259
  17.4 1.9 %copy.7 = bf16[1,128,2048]{2,1,0:T(8,128)(2,1)} copy(bf16[1,128,2048]{2,1,0:T(8,128)(2,1)} %shard_map.55) | data formatting | bytes 1048576

commit v2 on v1

--- a/solution.py
+++ b/solution.py
@@ -9,6 +9,7 @@
 from jax.sharding import PartitionSpec as P
 
 CONV = 4
+EDGE = CONV - 1
 gate_power = 8.0
 SUB = 8
 LANES = 128
@@ -16,6 +17,7 @@
 TINY = 1.2e-38
 LN2 = math.log(2.0)
 SMALL = 0.07
+NEAR = 4
 MESH = pl.DeviceIdType.MESH
 
 
@@ -29,8 +31,8 @@
     nsp, ndp, heads, block,
     x_hbm, cw_hbm, w_hbm, rate_hbm, pace_hbm, out_ref,
     x, cw, w, rate, pace_row, pace_mat, pace_perm, halo,
-    hloc, acum, ex_h, ex_a, stage, send_buf, recv_buf, carry,
-    load_sem, w_send, w_recv, halo_send, halo_recv, c_send, c_recv,
+    ends, hloc, acum, ex_h, ex_a, stage, send_buf, recv_buf, carry,
+    known, load_sem, w_send, w_recv, halo_send, halo_recv, c_send, c_recv,
 ):
     me = lax.axis_index("sp")
     d = lax.axis_index("dp")
@@ -43,9 +45,20 @@
 
     barrier = pltpu.get_barrier_semaphore()
 
-    @pl.loop(1, nsp)
-    def _(o):
-        pl.semaphore_signal(barrier, inc=1, device_id={"sp": lax.rem(me + o, nsp)}, device_id_type=MESH)
+    def at_distance(delta, ahead, then):
+        there = me + delta if ahead else me - delta
+
+        @pl.when(there < nsp if ahead else there >= 0)
+        def _():
+            then(there)
+
+    def greet(there):
+        pl.semaphore_signal(barrier, inc=1, device_id={"sp": there}, device_id_type=MESH)
+
+    near = range(1, min(NEAR, nsp - 1) + 1)
+    for delta in near:
+        for ahead in (True, False):
+            at_distance(delta, ahead, greet)
 
     @pl.loop(1, ndp)
     def _(o):
@@ -66,19 +79,31 @@
     def _():
         halo[...] = jnp.zeros_like(halo)
 
-    pl.semaphore_wait(barrier, nsp - 1 + ndp - 1)
+    rounds = []
+    while NEAR * 2 ** len(rounds) < nsp - 1:
+        rounds.append(NEAR * 2 ** len(rounds))
+
+    def tell(n):
+        for ahead in (True, False):
+            at_distance(rounds[n], ahead, lambda there, ahead=ahead: pl.semaphore_signal(
+                known.at[n, int(ahead)], inc=1, device_id={"sp": there}, device_id_type=MESH))
+
+    def learn(n):
+        for ahead in (True, False):
+            at_distance(rounds[n], ahead, lambda _, ahead=ahead: pl.semaphore_wait(
+                known.at[n, int(not ahead)], 1))
 
     w_copies = []
-    for o in range(1, ndp):
+    for slot in range(hl, heads):
+        o, own = slot // hl, slot % hl
         w_copies.append(pltpu.make_async_remote_copy(
-            src_ref=w_hbm,
-            dst_ref=w.at[:, pl.ds(o * hl, hl)],
-            send_sem=w_send.at[o],
-            recv_sem=w_recv.at[o],
+            src_ref=w.at[:, own],
+            dst_ref=w.at[:, slot],
+            send_sem=w_send.at[slot],
+            recv_sem=w_recv.at[slot],
             device_id={"dp": lax.rem(d - o + ndp, ndp)},
             device_id_type=MESH,
         ))
-    loads[0].wait()
     halo_copy = pltpu.make_async_remote_copy(
         src_ref=x.at[pl.ds(count - SUB, SUB)],
         dst_ref=halo,
@@ -87,15 +112,22 @@
         device_id={"sp": lax.rem(me + 1, nsp)},
         device_id_type=MESH,
     )
-
-    @pl.when(me < nsp - 1)
-    def _():
-        halo_copy.start()
-
-    for copy in w_copies:
-        copy.start()
-    for load in loads[1:]:
+    for load in loads:
         load.wait()
+
+    def meet_and_send():
+        reach = len(near)
+        peers = jnp.minimum(me, reach) + jnp.minimum(nsp - 1 - me, reach)
+        pl.semaphore_wait(barrier, peers + ndp - 1)
+
+        @pl.when(me < nsp - 1)
+        def _():
+            halo_copy.start()
+
+        for copy in w_copies:
+            copy.start()
+        if rounds:
+            tell(0)
 
     spread = jnp.broadcast_to(pace_row[...], (LANES, count)).T
     pace_mat[...] = spread
@@ -107,10 +139,6 @@
     gather = jnp.where(col == (row % SUB) * steps + row // SUB, 1.0, 0.0).astype(jnp.bfloat16)
     scatter = jnp.where(row == (col % SUB) * steps + col // SUB, 1.0, 0.0).astype(jnp.bfloat16)
     sub = lax.broadcasted_iota(jnp.int32, (SUB, block), 0)
-
-    @pl.when(me > 0)
-    def _():
-        halo_copy.wait_recv()
 
     def carry_copy(piece, src, dst):
         return pltpu.make_async_remote_copy(
@@ -122,27 +150,29 @@
             device_id_type=MESH,
         )
 
-    def one_slot(piece, at):
-        slot = piece * per + at
-        off = pl.multiple_of(lax.rem(d * hl + slot, heads) * block, block)
-        here = pl.ds(off, block)
-        xp = jnp.dot(gather, x[:, here], preferred_element_type=jnp.float32)
-        before = halo[:, here].astype(jnp.float32)
+    def take_halo():
+        @pl.when(me > 0)
+        def _():
+            halo_copy.wait_recv()
+
+        if rounds:
+            learn(len(rounds) - 1)
+
+    def columns(slot):
+        return pl.ds(pl.multiple_of(lax.rem(d * hl + slot, heads) * block, block), block)
+
+    def convolve(rows, here):
         taps = cw[:, here].astype(jnp.float32)
         taps = [jnp.broadcast_to(taps[k : k + 1], (SUB, block)) for k in range(CONV)]
-        rows = [xp[SUB * j : SUB * (j + 1)] for j in range(steps)]
-        early = []
-        for m in range(CONV - 1, 0, -1):
-            rolled = pltpu.roll(rows[steps - m], 1, 0)
-            edge = jnp.broadcast_to(before[SUB - m : SUB - m + 1], (SUB, block))
-            early.append(jnp.where(sub == 0, edge, rolled))
-        rows = early + rows
-        conv = []
-        for j in range(steps):
+        out = []
+        for j in range(len(rows) - EDGE):
             total = taps[0] * rows[j]
             for k in range(1, CONV):
                 total = total + taps[k] * rows[j + k]
-            conv.append(total)
+            out.append(total)
+        return out
+
+    def terms(conv, slot, here, first_step):
         conv = jnp.concatenate(conv, axis=0).astype(jnp.bfloat16)
         pre_r = jnp.dot(conv, w[0, slot], preferred_element_type=jnp.float32)
         pre_i = jnp.dot(conv, w[1, slot], preferred_element_type=jnp.float32)
@@ -151,11 +181,9 @@
         values = conv.astype(jnp.float32)
         factor = softplus_neg(rate[:, here]) * (gate_power / LN2)
         factor = jnp.broadcast_to(factor, (SUB, block))
-        h = None
-        for j in range(steps):
+        for j in range(conv.shape[0] // SUB):
             part = slice(SUB * j, SUB * (j + 1))
-            pace_j = pace_perm[j]
-            pace_j = jnp.concatenate([pace_j] * tiles, axis=1)
+            pace_j = jnp.concatenate([pace_perm[first_step + j]] * tiles, axis=1)
             r = 1.0 / (1.0 + jnp.exp(-pre_r[part]))
             i = 1.0 / (1.0 + jnp.exp(-pre_i[part]))
             q = pace_j * factor * r
@@ -164,13 +192,41 @@
             series = q * (c + q * (-c * c / 2 + q * (c**3 / 6 - q * (c**4 / 24))))
             gain = jnp.where(q < SMALL, series, 1.0 - a * a)
             b = gain * lax.rsqrt(jnp.maximum(gain, TINY)) * i * values[part]
+            yield a, b
+
+    def scan(pairs, slot, first_step):
+        h = total_a = None
+        for j, (a, b) in enumerate(pairs, first_step):
             if h is None:
                 h, total_a = b, a
             else:
                 h = a * h + b
                 total_a = total_a * a
+            part = slice(SUB * j, SUB * (j + 1))
             hloc[slot, part] = h
             acum[slot, part] = total_a
+
+    def main_slot(slot):
+        here = columns(slot)
+        xp = jnp.dot(gather, x[:, here], preferred_element_type=jnp.float32)
+        rows = [xp[SUB * j : SUB * (j + 1)] for j in range(steps)]
+        ends[slot] = jnp.concatenate(rows[steps - EDGE :] + rows[:EDGE], axis=0)
+        scan(terms(convolve(rows, here), slot, here, EDGE), slot, EDGE)
+
+    def edge_slot(piece, at):
+        slot = piece * per + at
+        here = columns(slot)
+        before = halo[:, here].astype(jnp.float32)
+        rows = [ends[slot, SUB * j : SUB * (j + 1)] for j in range(2 * EDGE)]
+        for j in range(EDGE):
+            edge = before[SUB - EDGE + j : SUB - EDGE + j + 1]
+            rows[j] = jnp.where(sub == 0, jnp.broadcast_to(edge, (SUB, block)), pltpu.roll(rows[j], 1, 0))
+        conv = convolve(rows, here)
+        scan(terms(conv, slot, here, 0), slot, 0)
+        edge_end = slice(SUB * (EDGE - 1), SUB * EDGE)
+        chunk_end = slice(SUB * (steps - 1), SUB * steps)
+        h = hloc[slot, chunk_end] + acum[slot, chunk_end] * hloc[slot, edge_end]
+        total_a = acum[slot, chunk_end] * acum[slot, edge_end]
         for shift in (1, 2, 4):
             inside = sub >= shift
             earlier_a = jnp.where(inside, pltpu.roll(total_a, shift, 0), 1.0)
@@ -185,20 +241,47 @@
             stage[pl.ds(at * tiles + t, 1), :] = log_a[SUB - 1 :, lanes]
             stage[pl.ds(SUB + at * tiles + t, 1), :] = h[SUB - 1 :, lanes]
 
-    for piece in range(pieces):
-        for o in range(1, ndp):
-            if piece * per <= o * hl < (piece + 1) * per:
-                w_copies[o - 1].wait_recv()
-
+    def main_slots(low, high):
+        for slot in range(max(hl, low), high):
+            w_copies[slot - hl].wait_recv()
+
+        @pl.loop(low, high)
+        def _(slot):
+            main_slot(slot)
+
+    def edge_and_send(piece):
         @pl.loop(0, per)
         def _(at):
-            one_slot(piece, at)
+            edge_slot(piece, at)
 
         send_buf[piece] = stage[...].astype(jnp.bfloat16)
 
         @pl.loop(me + 1, nsp)
         def _(dst):
             carry_copy(piece, me, dst).start()
+
+    half = per // 2
+    for piece in range(pieces):
+        low = piece * per
+        if piece == 0:
+            if hl > half:
+                main_slots(low, low + half)
+                meet_and_send()
+            else:
+                main_slots(low, low + hl)
+                meet_and_send()
+                main_slots(low + hl, low + half)
+            main_slots(low + half, low + per)
+            for n in range(1, len(rounds)):
+                learn(n - 1)
+                tell(n)
+        else:
+            main_slots(low, low + half)
+            if piece == 1:
+                take_halo()
+                edge_and_send(0)
+            main_slots(low + half, low + per)
+            edge_and_send(piece)
 
     def finish_slot(piece, at):
         slot = piece * per + at
@@ -211,8 +294,11 @@
             axis=1,
         )
         start = ex_h[slot] + ex_a[slot] * start
+        edge_end = slice(SUB * (EDGE - 1), SUB * EDGE)
+        later = hloc[slot, edge_end] + acum[slot, edge_end] * start
         states = [
-            hloc[slot, SUB * j : SUB * (j + 1)] + acum[slot, SUB * j : SUB * (j + 1)] * start
+            hloc[slot, SUB * j : SUB * (j + 1)]
+            + acum[slot, SUB * j : SUB * (j + 1)] * (start if j < EDGE else later)
             for j in range(steps)
         ]
         states = jnp.concatenate(states, axis=0).astype(jnp.bfloat16)
@@ -254,12 +340,12 @@
     heads = width // block
     pieces = width // PIECE
     f32, bf16 = jnp.float32, jnp.bfloat16
-    anywhere = pl.BlockSpec(memory_space=pl.ANY)
+    hbm = pl.BlockSpec(memory_space=pltpu.HBM)
     dma = pltpu.SemaphoreType.DMA
     return pl.pallas_call(
         functools.partial(kernel, nsp, ndp, heads, block),
-        out_shape=jax.ShapeDtypeStruct(inputs.shape, bf16),
-        in_specs=[anywhere] * 5,
+        out_shape=pltpu.VMEM(inputs.shape, bf16),
+        in_specs=[hbm] * 5,
         out_specs=pl.BlockSpec(memory_space=pltpu.VMEM),
         scratch_shapes=[
             pltpu.VMEM((count, width), bf16),
@@ -270,6 +356,7 @@
             pltpu.VMEM((count, LANES), f32),
             pltpu.VMEM((count // SUB, SUB, LANES), f32),
             pltpu.VMEM((SUB, width), bf16),
+            pltpu.VMEM((heads, 2 * EDGE * SUB, block), f32),
             pltpu.VMEM((heads, count, block), f32),
             pltpu.VMEM((heads, count, block), f32),
             pltpu.VMEM((heads, SUB, block), f32),
@@ -278,9 +365,10 @@
             pltpu.VMEM((pieces, 2 * SUB, LANES), bf16),
             pltpu.VMEM((nsp, pieces, 2 * SUB, LANES), bf16),
             pltpu.VMEM((SUB, LANES), f32),
+            pltpu.SemaphoreType.REGULAR((8, 2)),
             dma((5,)),
-            dma((ndp,)),
-            dma((ndp,)),
+            dma((heads,)),
+            dma((heads,)),
             dma((1,)),
             dma((1,)),
             dma((nsp, pieces)),

time: 19.5 us -> 16 us (0.82)
  Pallas kernels: 17.4 us -> 15 us
  local copies, waits for them, and re-layouts: 1.88 us -> 0.8 us
    pallas_call x1, Pallas kernels: 17.4 us -> 15 us  [body(): pl.pallas_call(functools.partial(kernel, nsp, ndp, heads, block), out_sha...]
    unnamed x1, local copies, waits for them, and re-layouts: 1.88 us -> 0.8 us
where the time goes in v2:
time: 16 us; the launch traced here: 15.8 us
  Pallas kernels  15 us (94%)
  local copies, waits for them, and re-layouts  0.8 us (5%)
    pallas_call x1, Pallas kernels, body(): pl.pallas_call(functools.partial(kernel, nsp, ndp, heads, block), out_sha...  15 us
    unnamed x1, local copies, waits for them, and re-layouts  0.8 us

profile of v2, /device:TPU:24, one launch (start us, length us, event | category | flops | bytes accessed | tf_op | source)
XLA Modules:
  0.0 15.8 jit_solution(8297102773078025367)
XLA Ops:
  0.0 15.0 %shard_map.55 = bf16[1,128,2048]{2,1,0:T(8,128)(2,1)S(1)} custom-call(bf16[1,128,2048]{2,1,0:T(8,128)(2,1)} %x_hbm.1, bf16[4,2048]{1,0:T(4,128)(2,1)} %cw_hbm.1, bf16[2,4,256,256]{3,2,1,0:T(8,128)(2,1)} %w_hbm.1, f32[1,2048]{1,0:T(1,128)} %bitcast.1, f32[1,2048]{1,0:T(1,128)} %pace_hbm.1), custom_call_target="tpu_custom_call" | custom-call | tf_op jit(solution)/shard_map/pallas_call | solution.py:345
  15.1 0.8 %copy.7 = bf16[1,128,2048]{2,1,0:T(8,128)(2,1)} copy(bf16[1,128,2048]{2,1,0:T(8,128)(2,1)S(1)} %shard_map.55) | data formatting | bytes 1048576

commit v3 on v2

--- a/solution.py
+++ b/solution.py
@@ -16,7 +16,8 @@
 PIECE = SUB * LANES
 TINY = 1.2e-38
 LN2 = math.log(2.0)
-SMALL = 0.07
+SMALL = 0.015
+SPLIT = 2
 NEAR = 4
 MESH = pl.DeviceIdType.MESH
 
@@ -155,9 +156,6 @@
         def _():
             halo_copy.wait_recv()
 
-        if rounds:
-            learn(len(rounds) - 1)
-
     def columns(slot):
         return pl.ds(pl.multiple_of(lax.rem(d * hl + slot, heads) * block, block), block)
 
@@ -176,8 +174,6 @@
         conv = jnp.concatenate(conv, axis=0).astype(jnp.bfloat16)
         pre_r = jnp.dot(conv, w[0, slot], preferred_element_type=jnp.float32)
         pre_i = jnp.dot(conv, w[1, slot], preferred_element_type=jnp.float32)
-        pre_r = pre_r.astype(jnp.bfloat16).astype(jnp.float32)
-        pre_i = pre_i.astype(jnp.bfloat16).astype(jnp.float32)
         values = conv.astype(jnp.float32)
         factor = softplus_neg(rate[:, here]) * (gate_power / LN2)
         factor = jnp.broadcast_to(factor, (SUB, block))
@@ -189,7 +185,7 @@
             q = pace_j * factor * r
             a = jnp.exp2(-q)
             c = 2.0 * LN2
-            series = q * (c + q * (-c * c / 2 + q * (c**3 / 6 - q * (c**4 / 24))))
+            series = q * (c + q * (c**3 / 6 * q - c * c / 2))
             gain = jnp.where(q < SMALL, series, 1.0 - a * a)
             b = gain * lax.rsqrt(jnp.maximum(gain, TINY)) * i * values[part]
             yield a, b
@@ -213,20 +209,37 @@
         ends[slot] = jnp.concatenate(rows[steps - EDGE :] + rows[:EDGE], axis=0)
         scan(terms(convolve(rows, here), slot, here, EDGE), slot, EDGE)
 
+    def with_halo(rows, here):
+        before = halo[:, here].astype(jnp.float32)
+        out = []
+        for j in range(EDGE):
+            edge = before[SUB - EDGE + j : SUB - EDGE + j + 1]
+            out.append(jnp.where(sub == 0, jnp.broadcast_to(edge, (SUB, block)), pltpu.roll(rows[j], 1, 0)))
+        return out
+
+    def full_slot(piece, at):
+        slot = piece * per + at
+        here = columns(slot)
+        xp = jnp.dot(gather, x[:, here], preferred_element_type=jnp.float32)
+        rows = [xp[SUB * j : SUB * (j + 1)] for j in range(steps)]
+        rows = with_halo(rows[steps - EDGE :], here) + rows
+        scan(terms(convolve(rows, here), slot, here, 0), slot, 0)
+        chunk_end = slice(SUB * (steps - 1), SUB * steps)
+        totals(slot, at, hloc[slot, chunk_end], acum[slot, chunk_end])
+
     def edge_slot(piece, at):
         slot = piece * per + at
         here = columns(slot)
-        before = halo[:, here].astype(jnp.float32)
         rows = [ends[slot, SUB * j : SUB * (j + 1)] for j in range(2 * EDGE)]
-        for j in range(EDGE):
-            edge = before[SUB - EDGE + j : SUB - EDGE + j + 1]
-            rows[j] = jnp.where(sub == 0, jnp.broadcast_to(edge, (SUB, block)), pltpu.roll(rows[j], 1, 0))
+        rows = with_halo(rows[:EDGE], here) + rows[EDGE:]
         conv = convolve(rows, here)
         scan(terms(conv, slot, here, 0), slot, 0)
         edge_end = slice(SUB * (EDGE - 1), SUB * EDGE)
         chunk_end = slice(SUB * (steps - 1), SUB * steps)
         h = hloc[slot, chunk_end] + acum[slot, chunk_end] * hloc[slot, edge_end]
-        total_a = acum[slot, chunk_end] * acum[slot, edge_end]
+        totals(slot, at, h, acum[slot, chunk_end] * acum[slot, edge_end])
+
+    def totals(slot, at, h, total_a):
         for shift in (1, 2, 4):
             inside = sub >= shift
             earlier_a = jnp.where(inside, pltpu.roll(total_a, shift, 0), 1.0)
@@ -241,20 +254,33 @@
             stage[pl.ds(at * tiles + t, 1), :] = log_a[SUB - 1 :, lanes]
             stage[pl.ds(SUB + at * tiles + t, 1), :] = h[SUB - 1 :, lanes]
 
-    def main_slots(low, high):
+    def wait_maps(low, high):
         for slot in range(max(hl, low), high):
             w_copies[slot - hl].wait_recv()
 
-        @pl.loop(low, high)
+    def main_slots(low, high):
+        wait_maps(low, high)
+
+        @pl.loop(low, high, unroll=True)
         def _(slot):
             main_slot(slot)
 
-    def edge_and_send(piece):
-        @pl.loop(0, per)
+    def edge_and_send(piece, split):
+        @pl.loop(0, split, unroll=True)
         def _(at):
             edge_slot(piece, at)
 
+        if split < per:
+            wait_maps(piece * per + split, piece * per + per)
+
+            @pl.loop(split, per, unroll=True)
+            def _(at):
+                full_slot(piece, at)
+
         send_buf[piece] = stage[...].astype(jnp.bfloat16)
+
+        if piece == 0 and rounds:
+            learn(len(rounds) - 1)
 
         @pl.loop(me + 1, nsp)
         def _(dst):
@@ -276,12 +302,13 @@
                 learn(n - 1)
                 tell(n)
         else:
-            main_slots(low, low + half)
+            ahead = SPLIT if piece == 1 else 0
+            if ahead:
+                main_slots(low, low + ahead)
             if piece == 1:
                 take_halo()
-                edge_and_send(0)
-            main_slots(low + half, low + per)
-            edge_and_send(piece)
+                edge_and_send(0, per)
+            edge_and_send(piece, ahead)
 
     def finish_slot(piece, at):
         slot = piece * per + at
@@ -295,7 +322,9 @@
         )
         start = ex_h[slot] + ex_a[slot] * start
         edge_end = slice(SUB * (EDGE - 1), SUB * EDGE)
-        later = hloc[slot, edge_end] + acum[slot, edge_end] * start
+        later = start
+        if piece == 0 or at < SPLIT:
+            later = hloc[slot, edge_end] + acum[slot, edge_end] * start
         states = [
             hloc[slot, SUB * j : SUB * (j + 1)]
             + acum[slot, SUB * j : SUB * (j + 1)] * (start if j < EDGE else later)
@@ -314,8 +343,7 @@
             got = recv_buf[src, piece].astype(jnp.float32)
             carry[...] = jnp.exp2(got[:SUB]) * carry[...] + got[SUB:]
 
-        @pl.loop(0, per)
-        def _(at):
+        for at in range(per):
             finish_slot(piece, at)
 
     for copy in w_copies:

time: 16 us -> 13.6 us (0.85)
  Pallas kernels: 15 us -> 12.7 us
    pallas_call x1, Pallas kernels: 15 us -> 12.7 us  [body(): pl.pallas_call(functools.partial(kernel, nsp, ndp, heads, block), out_sha...]
where the time goes in v3:
time: 13.6 us; the launch traced here: 13.5 us
  Pallas kernels  12.7 us (93%)
  local copies, waits for them, and re-layouts  0.8 us (6%)
    pallas_call x1, Pallas kernels, body(): pl.pallas_call(functools.partial(kernel, nsp, ndp, heads, block), out_sha...  12.7 us
    unnamed x1, local copies, waits for them, and re-layouts  0.8 us

profile of v3, /device:TPU:24, one launch (start us, length us, event | category | flops | bytes accessed | tf_op | source)
XLA Modules:
  0.0 13.5 jit_solution(4418263969072029118)
XLA Ops:
  0.0 12.7 %shard_map.55 = bf16[1,128,2048]{2,1,0:T(8,128)(2,1)S(1)} custom-call(bf16[1,128,2048]{2,1,0:T(8,128)(2,1)} %x_hbm.1, bf16[4,2048]{1,0:T(4,128)(2,1)} %cw_hbm.1, bf16[2,4,256,256]{3,2,1,0:T(8,128)(2,1)} %w_hbm.1, f32[1,2048]{1,0:T(1,128)} %bitcast.1, f32[1,2048]{1,0:T(1,128)} %pace_hbm.1), custom_call_target="tpu_custom_call" | custom-call | tf_op jit(solution)/shard_map/pallas_call | solution.py:373
  12.7 0.8 %copy.7 = bf16[1,128,2048]{2,1,0:T(8,128)(2,1)} copy(bf16[1,128,2048]{2,1,0:T(8,128)(2,1)S(1)} %shard_map.55) | data formatting | bytes 1048576

commit v4 on v3

--- a/solution.py
+++ b/solution.py
@@ -18,6 +18,7 @@
 LN2 = math.log(2.0)
 SMALL = 0.015
 SPLIT = 2
+FIRST = 1
 NEAR = 4
 MESH = pl.DeviceIdType.MESH
 
@@ -33,7 +34,7 @@
     x_hbm, cw_hbm, w_hbm, rate_hbm, pace_hbm, out_ref,
     x, cw, w, rate, pace_row, pace_mat, pace_perm, halo,
     ends, hloc, acum, ex_h, ex_a, stage, send_buf, recv_buf, carry,
-    known, load_sem, w_send, w_recv, halo_send, halo_recv, c_send, c_recv,
+    known, load_sem, map_sem, w_send, w_recv, halo_send, halo_recv, c_send, c_recv,
 ):
     me = lax.axis_index("sp")
     d = lax.axis_index("dp")
@@ -68,12 +69,15 @@
     first = pl.multiple_of(me * count, count)
     loads = [
         pltpu.make_async_copy(x_hbm.at[0], x, load_sem.at[0]),
-        pltpu.make_async_copy(w_hbm, w.at[:, pl.ds(0, hl)], load_sem.at[1]),
-        pltpu.make_async_copy(cw_hbm, cw, load_sem.at[2]),
-        pltpu.make_async_copy(rate_hbm, rate, load_sem.at[3]),
-        pltpu.make_async_copy(pace_hbm.at[:, pl.ds(first, count)], pace_row, load_sem.at[4]),
+        pltpu.make_async_copy(cw_hbm, cw, load_sem.at[1]),
+        pltpu.make_async_copy(rate_hbm, rate, load_sem.at[2]),
+        pltpu.make_async_copy(pace_hbm.at[:, pl.ds(first, count)], pace_row, load_sem.at[3]),
     ]
-    for load in loads:
+    map_loads = [
+        pltpu.make_async_copy(w_hbm.at[:, own], w.at[:, own], map_sem.at[own])
+        for own in range(hl)
+    ]
+    for load in loads + map_loads:
         load.start()
 
     @pl.when(me == 0)
@@ -290,17 +294,19 @@
     for piece in range(pieces):
         low = piece * per
         if piece == 0:
-            if hl > half:
-                main_slots(low, low + half)
-                meet_and_send()
-            else:
-                main_slots(low, low + hl)
-                meet_and_send()
-                main_slots(low + hl, low + half)
-            main_slots(low + half, low + per)
+            begun = low + min(hl, FIRST)
+            for load in map_loads[:begun]:
+                load.wait()
+            middle = begun + (low + per - begun) // 2
+            main_slots(low, begun)
+            for load in map_loads[begun:]:
+                load.wait()
+            meet_and_send()
+            main_slots(begun, middle)
             for n in range(1, len(rounds)):
                 learn(n - 1)
                 tell(n)
+            main_slots(middle, low + per)
         else:
             ahead = SPLIT if piece == 1 else 0
             if ahead:
@@ -366,6 +372,7 @@
     _, count, width = inputs.shape
     block = gate_weight.shape[-1]
     heads = width // block
+    hl = heads // ndp
     pieces = width // PIECE
     f32, bf16 = jnp.float32, jnp.bfloat16
     hbm = pl.BlockSpec(memory_space=pltpu.HBM)
@@ -394,7 +401,8 @@
             pltpu.VMEM((nsp, pieces, 2 * SUB, LANES), bf16),
             pltpu.VMEM((SUB, LANES), f32),
             pltpu.SemaphoreType.REGULAR((8, 2)),
-            dma((5,)),
+            dma((4,)),
+            dma((hl,)),
             dma((heads,)),
             dma((heads,)),
             dma((1,)),

time: 13.6 us -> 13.2 us (0.971)
  Pallas kernels: 12.7 us -> 12.3 us
    pallas_call x1, Pallas kernels: 12.7 us -> 12.3 us  [body(): pl.pallas_call(functools.partial(kernel, nsp, ndp, heads, block), out_sha...]
where the time goes in v4:
time: 13.2 us; the launch traced here: 13.1 us
  Pallas kernels  12.3 us (93%)
  local copies, waits for them, and re-layouts  0.8 us (6%)
    pallas_call x1, Pallas kernels, body(): pl.pallas_call(functools.partial(kernel, nsp, ndp, heads, block), out_sha...  12.3 us
    unnamed x1, local copies, waits for them, and re-layouts  0.8 us

profile of v4, /device:TPU:24, one launch (start us, length us, event | category | flops | bytes accessed | tf_op | source)
XLA Modules:
  0.0 13.1 jit_solution(13319885940097721536)
XLA Ops:
  0.0 12.3 %shard_map.55 = bf16[1,128,2048]{2,1,0:T(8,128)(2,1)S(1)} custom-call(bf16[1,128,2048]{2,1,0:T(8,128)(2,1)} %x_hbm.1, bf16[4,2048]{1,0:T(4,128)(2,1)} %cw_hbm.1, bf16[2,4,256,256]{3,2,1,0:T(8,128)(2,1)} %w_hbm.1, f32[1,2048]{1,0:T(1,128)} %bitcast.1, f32[1,2048]{1,0:T(1,128)} %pace_hbm.1), custom_call_target="tpu_custom_call" | custom-call | tf_op jit(solution)/shard_map/pallas_call | solution.py:380
  12.3 0.8 %copy.7 = bf16[1,128,2048]{2,1,0:T(8,128)(2,1)} copy(bf16[1,128,2048]{2,1,0:T(8,128)(2,1)S(1)} %shard_map.55) | data formatting | bytes 1048576
